TPU v7x, 32 devices: a whole 2x2x4 slice. The times are simulated.
32 devices in a mesh: grp: 2 (over y), ep: 4 (over z), tp: 4 (over x, core).
Axes of the slice: x: 2, y: 2, z: 4, core: 2. Of those that a mesh axis runs over, the one named last changes fastest.
Arguments:
- queries: bfloat16 [4096, 768], P(('grp', 'ep'), 'tp'), parts along dimension 0, may hold values from -6 to 6
- key_value: bfloat16 [4096, 4, 128], P(('grp', 'ep'), 'tp'), parts along dimension 0, may hold values from -6 to 6
- key_bias: bfloat16 [4, 4096], P('tp', ('grp', 'ep')), parts along dimension 1, may hold values from -20 to 0
- out_weight: bfloat16 [768, 2048], P('tp'), may hold values from -0.75 to 0.75
- expert_input: bfloat16 [4096, 2048], P(('grp', 'ep', 'tp')), parts along dimension 0, may hold values from -6 to 6
- norm_gain: float32 [2048], replicated, may hold values from 0.1 to 1.9
- routes: int32 [4096, 4], P(('grp', 'ep', 'tp')), parts along dimension 0, may hold values from 0 to 15, as said below
- route_weights: float32 [4096, 4], P(('grp', 'ep', 'tp')), parts along dimension 0, may hold values from 0.2 to 1
- gate_weight: bfloat16 [16, 2048, 512], P(('ep', 'tp')), may hold values from -0.125 to 0.125
- up_weight: bfloat16 [16, 2048, 512], P(('ep', 'tp')), may hold values from -0.125 to 0.125
- down_weight: bfloat16 [16, 512, 2048], P(('ep', 'tp')), may hold values from -0.25 to 0.25
- shared_gate: bfloat16 [2048, 256], replicated, may hold values from -0.125 to 0.125
- shared_up: bfloat16 [2048, 256], replicated, may hold values from -0.125 to 0.125
- shared_down: bfloat16 [256, 2048], replicated, may hold values from -0.375 to 0.375
Outputs:
- mixer_output: bfloat16 [4096, 2048], P(('grp', 'ep', 'tp')), parts along dimension 0
- expert_output: bfloat16 [4096, 2048], P(('grp', 'ep', 'tp')), parts along dimension 0
There are 2 independent parts, one for each index of `grp`. A program takes and returns all parts, laid end to end along the dimension named above; an argument that names none is the same for every part. Nothing has to cross between parts.
Inputs may be any that keep to these rules, and one draw needn't show every extreme that they name: `routes`: each row names 4 different experts. Among the 128 rows of one device no expert is named more than 48 times, and in every draw one expert is named exactly 48 times in the rows of every device.
All inputs are finite; a program needn't handle non-finite values.
Results may differ from a plain program's by a relative error of at most 0.009.
Values may be sent and summed in bfloat16 or wider, within the bound.
No kernel may reach another device: no remote copies, remote signals or barrier semaphores. Data moves between devices by JAX's collectives and lax.ppermute only.
A program may use at most 128 MiB of HBM per device.

v0:
```python
import jax
import jax.numpy as jnp
from jax import lax
from jax.sharding import PartitionSpec as P


def passed_along(block, axis, distance):
    devices = range(lax.axis_size(axis))
    route = [(i - distance, i) for i in devices if i - distance in devices]
    return lax.ppermute(block, axis, route)


def piece_update(running, query_rows, key_rows, value_rows, key_offset, allowed):
    totals, kept_sum = running
    logits = (
        jnp.einsum("sgrd,kgd->grsk", query_rows, key_rows, preferred_element_type=jnp.float32)
        * 0.125
    )
    logits = logits + key_offset.astype(jnp.float32)[:, None, None, :]
    log_keep = jnp.where(allowed, -jax.nn.softplus(logits), 0.0)
    log_after = lax.cumsum(log_keep, axis=3, reverse=True) - log_keep
    weights = jnp.where(
        allowed, jnp.exp(jax.nn.log_sigmoid(logits) + log_after + kept_sum[..., None]), 0.0
    )
    weights = weights.astype(jnp.bfloat16)
    totals = totals + jnp.einsum(
        "grsk,kgd->grsd", weights, value_rows, preferred_element_type=jnp.float32
    )
    return (totals, kept_sum + jnp.sum(log_keep, axis=3))


def mixer_half(queries, key_value, key_bias, out_weight):
    span_rows, key_groups, pair_width = key_value.shape
    head_dim = pair_width // 2
    per_group = queries.shape[1] // (key_groups * head_dim)
    query_rows = queries.reshape(span_rows, key_groups, per_group, head_dim)
    axis_size = lax.axis_size("ep")
    chain_length = axis_size // max(1, axis_size // 4)
    device_place = lax.axis_index("ep")
    chain_place = jnp.minimum((device_place + 2) % chain_length, device_place)
    positions = jnp.arange(span_rows, dtype=jnp.int32)
    strict_mask = positions[None, :] < positions[:, None]
    full_mask = jnp.ones((span_rows, span_rows), dtype=bool)
    initial = (
        jnp.zeros((key_groups, per_group, span_rows, head_dim), jnp.float32),
        jnp.zeros((key_groups, per_group, span_rows), jnp.float32),
    )
    running = piece_update(
        initial,
        query_rows,
        key_value[..., :head_dim],
        key_value[..., head_dim:],
        key_bias,
        strict_mask,
    )

    def advance(distance, loop_state):
        current, visiting_keys, visiting_bias = loop_state
        visiting_keys, visiting_bias = passed_along((visiting_keys, visiting_bias), "ep", 1)

        def include(earlier_state):
            return piece_update(
                earlier_state,
                query_rows,
                visiting_keys[..., :head_dim],
                visiting_keys[..., head_dim:],
                visiting_bias,
                full_mask,
            )

        def skip(earlier_state):
            return earlier_state

        current = lax.cond(distance <= chain_place, include, skip, current)
        return (current, visiting_keys, visiting_bias)

    running, _, _ = lax.fori_loop(1, chain_length, advance, (running, key_value, key_bias))
    attended = running[0].astype(jnp.bfloat16)
    projection = out_weight.reshape(key_groups, per_group, head_dim, out_weight.shape[1])
    return lax.psum_scatter(
        jnp.einsum(
            "grsd,grde->se", attended, projection, preferred_element_type=jnp.float32
        ).astype(jnp.bfloat16),
        "tp",
        scatter_dimension=0,
        tiled=True,
    )


def expert_rows(arrived, gate_weight, up_weight, down_weight):
    sources, capacity, model_width = arrived.shape
    flat_rows = arrived.reshape(sources * capacity, model_width)
    gate_part = jnp.dot(flat_rows, gate_weight[0], preferred_element_type=jnp.float32)
    up_part = jnp.dot(flat_rows, up_weight[0], preferred_element_type=jnp.float32)
    hidden = (jax.nn.silu(gate_part) * up_part).astype(jnp.bfloat16)
    result = jnp.dot(hidden, down_weight[0], preferred_element_type=jnp.float32).astype(
        jnp.bfloat16
    )
    return result.reshape(sources, capacity, model_width)


def experts_half(
    expert_input,
    norm_gain,
    routes,
    route_weights,
    gate_weight,
    up_weight,
    down_weight,
    shared_gate,
    shared_up,
    shared_down,
):
    tokens, top_count = routes.shape
    model_width = expert_input.shape[1]
    ep_count = lax.axis_size("ep")
    tp_count = lax.axis_size("tp")
    experts = ep_count * tp_count
    capacity = max(2, 3 * tokens * top_count // (2 * experts))
    widened = expert_input.astype(jnp.float32)
    normed = (
        widened * lax.rsqrt(jnp.mean(widened * widened, axis=-1, keepdims=True) + 1e-06) * norm_gain
    ).astype(jnp.bfloat16)
    flat_routes = routes.reshape(-1)
    one_hot = (flat_routes[:, None] == jnp.arange(experts, dtype=jnp.int32)[None, :]).astype(
        jnp.int32
    )
    before = jnp.cumsum(one_hot, axis=0) - one_hot
    slot_index = jnp.sum(before * one_hot, axis=1)
    target = flat_routes * capacity + slot_index
    picker = (jnp.arange(experts * capacity, dtype=jnp.int32)[:, None] == target[None, :]).astype(
        jnp.bfloat16
    )
    picker = jnp.sum(picker.reshape(experts * capacity, tokens, top_count), axis=2)
    outgoing = jnp.dot(picker, normed, preferred_element_type=jnp.float32).astype(jnp.bfloat16)
    outgoing = outgoing.reshape(experts, capacity, model_width)
    came_back = lax.all_to_all(
        expert_rows(
            lax.all_to_all(outgoing, ("ep", "tp"), split_axis=0, concat_axis=0, tiled=True),
            gate_weight,
            up_weight,
            down_weight,
        ),
        ("ep", "tp"),
        split_axis=0,
        concat_axis=0,
        tiled=True,
    )
    back_rows = came_back.reshape(experts * capacity, model_width)
    picked = jnp.take(back_rows, target, axis=0).reshape(tokens, top_count, model_width)
    routed = jnp.sum(picked.astype(jnp.float32) * route_weights[:, :, None], axis=1)
    shared_hidden = (
        jax.nn.silu(jnp.dot(normed, shared_gate, preferred_element_type=jnp.float32))
        * jnp.dot(normed, shared_up, preferred_element_type=jnp.float32)
    ).astype(jnp.bfloat16)
    shared_term = jnp.dot(shared_hidden, shared_down, preferred_element_type=jnp.float32)
    return (routed + shared_term).astype(jnp.bfloat16)


def per_device(
    queries,
    key_value,
    key_bias,
    out_weight,
    expert_input,
    norm_gain,
    routes,
    route_weights,
    gate_weight,
    up_weight,
    down_weight,
    shared_gate,
    shared_up,
    shared_down,
):
    mixer_output = mixer_half(queries, key_value, key_bias, out_weight)
    expert_output = experts_half(
        expert_input,
        norm_gain,
        routes,
        route_weights,
        gate_weight,
        up_weight,
        down_weight,
        shared_gate,
        shared_up,
        shared_down,
    )
    return (mixer_output, expert_output)


def solution(mesh):
    placed = (
        P(("grp", "ep"), "tp"),
        P(("grp", "ep"), "tp", None),
        P("tp", ("grp", "ep")),
        P("tp", None),
        P(("grp", "ep", "tp"), None),
        P(),
        P(("grp", "ep", "tp"), None),
        P(("grp", "ep", "tp"), None),
        P(("ep", "tp"), None, None),
        P(("ep", "tp"), None, None),
        P(("ep", "tp"), None, None),
        P(),
        P(),
        P(),
    )
    return jax.shard_map(
        per_device,
        mesh=mesh,
        in_specs=placed,
        out_specs=(P(("grp", "ep", "tp"), None), P(("grp", "ep", "tp"), None)),
        check_vma=False,
    )
```

profile of v0, /device:TPU:0, one launch (start us, length us, event | category | flops | bytes accessed | tf_op | source)
XLA Modules:
  0.0 265.7 jit_solution(3107453401127544733)
XLA Ops:
  7.2 0.8 copy.101
  8.0 0.8 copy.66
  9.0 1.2 reduce-window.26
  10.7 0.7 compare_and_fusion
  11.6 1.2 fusion.57
  12.8 2.1 convolution_convert_fusion.1
  15.0 76.9 %all_to_all.10 = bf16[16,48,2048]{2,1,0:T(8,128)(2,1)S(1)} all-to-all(bf16[16,48,2048]{2,1,0:T(8,128)(2,1)S(1)} %bitcast.200), channel_id=1, replica_groups=mesh['grp'=2,'ep'=4,'tp'=4] {'ep','tp'}, dimensions={0} | all-to-all | bytes 6291456 | tf_op jit(solution)/shard_map/all_to_all | solution.py:139
  91.9 1.7 copy-done.2
  93.6 2.9 %fusion.46 = f32[768,512]{1,0:T(8,128)} fusion(bf16[768,2048]{1,0:T(8,128)(2,1)S(1)} %bitcast.203, bf16[1,2048,512]{2,1,0:T(8,128)(2,1)S(1)} %copy-done.7), kind=kOutput, calls=%fused_computation.65 | convolution fusion | flops 1610612736 | bytes 6815744 | tf_op jit(solution)/shard_map/dot_general | solution.py:93
  96.6 8.1 %convolution_convert_fusion = bf16[768,2048]{1,0:T(8,128)(2,1)} fusion(bf16[1,512,2048]{2,1,0:T(8,128)(2,1)S(1)} %copy-done, f32[768,512]{1,0:T(8,128)} %fusion.46, bf16[768,2048]{1,0:T(8,128)(2,1)} %bitcast.204, bf16[1,2048,512]{2,1,0:T(8,128)(2,1)} %param.27), kind=kOutput, calls=%fused_computation.39 | convolution fusion | flops 3225157632 | bytes 12058624 | tf_op jit(solution)/shard_map/dot_general | solution.py:96
  104.7 5.4 %all-to-all-start.1 = ((bf16[16,48,2048]{2,1,0:T(8,128)(2,1)}), bf16[16,48,2048]{2,1,0:T(8,128)(2,1)}, u32[]{:S(2)}, u32[]{:S(2)}) async-start(bf16[16,48,2048]{2,1,0:T(8,128)(2,1)} %bitcast.201), calls=%async_computation.2 | async-start | bytes 6291456 | tf_op jit(solution)/shard_map/all_to_all | solution.py:137
  110.6 4.1 %fusion.79 = (f32[3,512]{1,0:T(4,128)S(1)}, f32[1,3,512,512]{2,3,1,0:T(8,128)S(1)}, f32[512,512,3]{1,0,2:T(8,128)}) fusion(f32[512]{0:T(512)S(1)} %bitcast.211, pred[512,512]{0,1:T(8,128)(4,1)S(1)} %iota_compare_fusion.1, bf16[512,3,64]{0,2,1:T(8,128)(2,1)S(1)} %bitcast.214, bf16[512,1,128]{0,2,1:T(8,128)(2,1)S(1)} %copy.60), kind=kOutput, calls=%fused_computation.113 | convolution fusion | flops 109312512 | bytes 6823936 | tf_op jit(solution)/shard_map/sgrd,kgd->grsk/dot_general | solution.py:16
  114.7 14.9 %fusion.40 = f32[1,3,512,4,128]{2,3,4,1,0:T(4,128)S(1)} fusion(f32[1,3,512,4,128]{2,4,3,1,0:T(8,128)S(1)} %bitcast.202), kind=kOutput, calls=%fused_computation.58 | output fusion | flops 99876864 | bytes 6291456 | tf_op jit(solution)/shard_map/reduce-window.2
  129.6 2.6 copy.62
  132.3 6.8 %fusion.32 = bf16[1,3,512,512]{2,3,1,0:T(8,128)(2,1)S(1)} fusion(f32[1,3,512,4,128]{2,4,3,1,0:T(8,128)} %copy.62, f32[512,512,3]{1,0,2:T(8,128)} %get-tuple-element.201, f32[3,512,4]{1,2,0:T(4,128)S(1)} %slice_bitcast_fusion.6, f32[512]{0:T(512)S(1)} %bitcast.212, pred[512,512]{0,1:T(8,128)(4,1)S(1)} %iota_compare_fusion.1), kind=kLoop, calls=%fused_computation.45 | loop fusion | flops 18087936 | bytes 8153088 | tf_op jit(solution)/shard_map/convert_element_type | solution.py:25
  139.5 84.5 %while.19 = (s32[]{:T(128)}, f32[1,3,512,64]{2,3,1,0:T(8,128)S(1)}, f32[1,3,512]{2,1,0:T(4,128)S(1)}, bf16[512,1,128]{0,2,1:T(8,128)(2,1)S(1)}, bf16[1,512]{1,0:...) while((s32[]{:T(128)}, f32[1,3,512,64]{2,3,1,0:T(8,128)S(1)}, ...), condition=%wide.region_9.10_spmd, body=%wide.region_3.0_spmd.sunk | while | flops 326492672 | bytes 30434568 | solution.py:77
  139.7 3.8 %collective-permute-start = (bf16[512,1,128]{0,2,1:T(8,128)(2,1)S(1)}, bf16[512,1,128]{0,2,1:T(8,128)(2,1)S(1)}, u32[]{:S(2)}, u32[]{:S(2)}) collective-permute-start(bf16[512,1,128]{0,2,1:T(8,128)(2,1)S(1)} %get-tuple-element.264), channel_id=1, source_target_pairs={{0,4},{4,8},{8,12},{1,5},{5,9},{9,13},{2,6},{6,10},{10,14},{3,7},{... | collective-permute-start | bytes 393224 | tf_op jit(solution)/shard_map/while/body/eval_jaxpr/ppermute | solution.py:10
  143.5 3.4 %collective-permute-start.1 = (bf16[1,512]{1,0:T(2,128)(2,1)S(1)}, bf16[1,512]{1,0:T(2,128)(2,1)S(1)}, u32[]{:S(2)}, u32[]{:S(2)}) collective-permute-start(bf16[1,512]{1,0:T(2,128)(2,1)S(1)} %get-tuple-element.265), channel_id=1, source_target_pairs={{0,4},{4,8},{8,12},{1,5},{5,9},{9,13},{2,6},{6,10},{10,14},{3,7},{... | collective-permute-start | bytes 3080 | tf_op jit(solution)/shard_map/while/body/eval_jaxpr/ppermute | solution.py:10
  146.8 17.8 %collective-permute-done.1 = bf16[1,512]{1,0:T(2,128)(2,1)S(1)} collective-permute-done((bf16[1,512]{1,0:T(2,128)(2,1)S(1)}, bf16[1,512]{1,0:T(2,128)(2,1)S(1)}, u32[]{:S(2)}, u32[]{:S(2)}) %collective-permute-start.1) | collective-permute-done | bytes 1056 | tf_op jit(solution)/shard_map/while/body/eval_jaxpr/ppermute | solution.py:10
  164.7 48.4 %collective-permute-start = (bf16[512,1,128]{0,2,1:T(8,128)(2,1)S(1)}, bf16[512,1,128]{0,2,1:T(8,128)(2,1)S(1)}, u32[]{:S(2)}, u32[]{:S(2)}) collective-permute-start(bf16[512,1,128]{0,2,1:T(8,128)(2,1)S(1)} %get-tuple-element.264), channel_id=1, source_target_pairs={{0,4},{4,8},{8,12},{1,5},{5,9},{9,13},{2,6},{6,10},{10,14},{3,7},{... | collective-permute-start | bytes 393224 | tf_op jit(solution)/shard_map/while/body/eval_jaxpr/ppermute | solution.py:10
  213.1 1.9 collective-permute-start.1
  215.0 1.3 collective-permute-done.1
  216.4 4.2 %collective-permute-start = (bf16[512,1,128]{0,2,1:T(8,128)(2,1)S(1)}, bf16[512,1,128]{0,2,1:T(8,128)(2,1)S(1)}, u32[]{:S(2)}, u32[]{:S(2)}) collective-permute-start(bf16[512,1,128]{0,2,1:T(8,128)(2,1)S(1)} %get-tuple-element.264), channel_id=1, source_target_pairs={{0,4},{4,8},{8,12},{1,5},{5,9},{9,13},{2,6},{6,10},{10,14},{3,7},{... | collective-permute-start | bytes 393224 | tf_op jit(solution)/shard_map/while/body/eval_jaxpr/ppermute | solution.py:10
  220.6 1.9 collective-permute-start.1
  222.5 1.3 collective-permute-done.1
  224.1 3.3 %bitcast_convert_fusion = bf16[512,2048]{1,0:T(8,128)(2,1)} fusion(bf16[3,64,2048]{2,1,0:T(8,128)(2,1)} %bitcast.213, f32[1,3,512,64]{2,3,1,0:T(8,128)S(1)} %get-tuple-element.151), kind=kOutput, calls=%fused_computation.37 | convolution fusion | flops 403800064 | bytes 3276800 | tf_op jit(solution)/shard_map/grsd,grde->se/dot_general | solution.py:81
  227.9 1.6 fusion.82
  229.5 7.6 %gather_fusion = bf16[512,2048]{1,0:T(8,128)(2,1)} fusion(bf16[768,2048]{1,0:T(8,128)(2,1)} %bitcast.44, s32[1024]{0:T(1024)S(1)} %pad_clamp_fusion), kind=kCustom, calls=%fused_computation | custom fusion | bytes 4196352 | tf_op jit(solution)/shard_map/jit(_take)/gather | solution.py:150
  237.1 4.1 %gather.7 = bf16[128,4,2048]{2,1,0:T(4,128)(2,1)} reshape(bf16[512,2048]{1,0:T(8,128)(2,1)} %gather_fusion) | data formatting | bytes 4194304 | tf_op jit(solution)/shard_map/jit(_take)/gather | solution.py:150
  241.2 6.6 %multiply_reduce_fusion = f32[128,2048]{1,0:T(8,128)} fusion(f32[128,4]{1,0:T(8,128)S(1)} %copy.72, bf16[128,4,2048]{2,1,0:T(4,128)(2,1)} %gather.7, pred[128,4]{1,0:T(8,128)(4,1)S(1)} %copy.70), kind=kLoop, calls=%fused_computation.38 | loop fusion | flops 3932160 | bytes 3148288 | tf_op jit(solution)/shard_map/reduce_sum | solution.py:151
  247.8 3.5 %fusion.42 = bf16[128,2048]{1,0:T(8,128)(2,1)} fusion(f32[128,2048]{1,0:T(8,128)} %multiply_reduce_fusion, bf16[256,2048]{1,0:T(8,128)(2,1)} %param.31, bf16[2048,256]{1,0:T(8,128)(2,1)} %param.30, f32[128,256]{1,0:T(8,128)S(1)} %fusion.82, bf16[128,2048]{1,0:T(8,128)(2,1)S(1)} %copy-done.1, f32[2048]{0:T(1024)S(1)} %copy-done.4, f32[128]{0:T(128)S(1)} %add_rsqrt_fusion), kind=kOutput, calls=%fused_computation.61 | convolution fusion | flops 270204928 | bytes 4334080 | tf_op jit(solution)/shard_map/dot_general | solution.py:156
  251.3 7.4 %reduce-scatter.2.cloned.1.call-done = bf16[128,2048]{1,0:T(8,128)(2,1)} async-done(((bf16[512,2048]{1,0:T(8,128)(2,1)}), bf16[128,2048]{1,0:T(8,128)(2,1)}) %reduce-scatter.2.cloned.1.call-update) | async-done | bytes 524304 | tf_op jit(solution)/shard_map/reduce_scatter | solution.py:80
  (57 shorter events, 2.4 us)
Async XLA Ops:
  7.2 89.4 %copy-start = (bf16[1,512,2048]{2,1,0:T(8,128)(2,1)S(1)}, bf16[1,512,2048]{2,1,0:T(8,128)(2,1)}, u32[]{:S(2)}) copy-start(bf16[1,512,2048]{2,1,0:T(8,128)(2,1)} %param.28) | copy-start | bytes 6291460
  15.0 78.7 %copy-start.7 = (bf16[1,2048,512]{2,1,0:T(8,128)(2,1)S(1)}, bf16[1,2048,512]{2,1,0:T(8,128)(2,1)}, u32[]{:S(2)}) copy-start(bf16[1,2048,512]{2,1,0:T(8,128)(2,1)} %param.26) | copy-start | bytes 6291460
  91.9 1.7 copy-start.2
  104.7 5.6 %copy-start.3 = (bf16[512,1,128]{2,0,1:T(8,128)(2,1)S(1)}, bf16[512,1,128]{2,0,1:T(8,128)(2,1)}, u32[]{:S(2)}) copy-start(bf16[512,1,128]{2,0,1:T(8,128)(2,1)} %param.19) | copy-start | bytes 393220
  104.7 5.9 %copy-start.8 = (bf16[512,192]{0,1:T(8,128)(2,1)S(1)}, bf16[512,192]{0,1:T(8,128)(2,1)}, u32[]{:S(2)}) copy-start(bf16[512,192]{0,1:T(8,128)(2,1)} %param.18) | copy-start | bytes 589828
  104.7 124.8 %all-to-all-start.1 = ((bf16[16,48,2048]{2,1,0:T(8,128)(2,1)}), bf16[16,48,2048]{2,1,0:T(8,128)(2,1)}, u32[]{:S(2)}, u32[]{:S(2)}) async-start(bf16[16,48,2048]{2,1,0:T(8,128)(2,1)} %bitcast.201), calls=%async_computation.2 | async-start | bytes 6291456 | tf_op jit(solution)/shard_map/all_to_all | solution.py:137
  110.1 148.5 %reduce-scatter.2.cloned.1.call-start = ((), (), s32[]{:S(2)}) async-start(), calls=%async_computation.3 | async-start | bytes 2621440 | tf_op jit(solution)/shard_map/reduce_scatter | solution.py:80
  139.7 25.0 %collective-permute-start = (bf16[512,1,128]{0,2,1:T(8,128)(2,1)S(1)}, bf16[512,1,128]{0,2,1:T(8,128)(2,1)S(1)}, u32[]{:S(2)}, u32[]{:S(2)}) collective-permute-start(bf16[512,1,128]{0,2,1:T(8,128)(2,1)S(1)} %get-tuple-element.264), channel_id=1, source_target_pairs={{0,4},{4,8},{8,12},{1,5},{5,9},{9,13},{2,6},{6,10},{10,14},{3,7},{... | collective-permute-start | bytes 393224 | tf_op jit(solution)/shard_map/while/body/eval_jaxpr/ppermute | solution.py:10
  143.5 21.2 %collective-permute-start.1 = (bf16[1,512]{1,0:T(2,128)(2,1)S(1)}, bf16[1,512]{1,0:T(2,128)(2,1)S(1)}, u32[]{:S(2)}, u32[]{:S(2)}) collective-permute-start(bf16[1,512]{1,0:T(2,128)(2,1)S(1)} %get-tuple-element.265), channel_id=1, source_target_pairs={{0,4},{4,8},{8,12},{1,5},{5,9},{9,13},{2,6},{6,10},{10,14},{3,7},{... | collective-permute-start | bytes 3080 | tf_op jit(solution)/shard_map/while/body/eval_jaxpr/ppermute | solution.py:10
  164.7 51.6 %collective-permute-start = (bf16[512,1,128]{0,2,1:T(8,128)(2,1)S(1)}, bf16[512,1,128]{0,2,1:T(8,128)(2,1)S(1)}, u32[]{:S(2)}, u32[]{:S(2)}) collective-permute-start(bf16[512,1,128]{0,2,1:T(8,128)(2,1)S(1)} %get-tuple-element.264), channel_id=1, source_target_pairs={{0,4},{4,8},{8,12},{1,5},{5,9},{9,13},{2,6},{6,10},{10,14},{3,7},{... | collective-permute-start | bytes 393224 | tf_op jit(solution)/shard_map/while/body/eval_jaxpr/ppermute | solution.py:10
  213.1 3.2 %collective-permute-start.1 = (bf16[1,512]{1,0:T(2,128)(2,1)S(1)}, bf16[1,512]{1,0:T(2,128)(2,1)S(1)}, u32[]{:S(2)}, u32[]{:S(2)}) collective-permute-start(bf16[1,512]{1,0:T(2,128)(2,1)S(1)} %get-tuple-element.265), channel_id=1, source_target_pairs={{0,4},{4,8},{8,12},{1,5},{5,9},{9,13},{2,6},{6,10},{10,14},{3,7},{... | collective-permute-start | bytes 3080 | tf_op jit(solution)/shard_map/while/body/eval_jaxpr/ppermute | solution.py:10
  216.4 7.4 %collective-permute-start = (bf16[512,1,128]{0,2,1:T(8,128)(2,1)S(1)}, bf16[512,1,128]{0,2,1:T(8,128)(2,1)S(1)}, u32[]{:S(2)}, u32[]{:S(2)}) collective-permute-start(bf16[512,1,128]{0,2,1:T(8,128)(2,1)S(1)} %get-tuple-element.264), channel_id=1, source_target_pairs={{0,4},{4,8},{8,12},{1,5},{5,9},{9,13},{2,6},{6,10},{10,14},{3,7},{... | collective-permute-start | bytes 393224 | tf_op jit(solution)/shard_map/while/body/eval_jaxpr/ppermute | solution.py:10
  220.6 3.2 %collective-permute-start.1 = (bf16[1,512]{1,0:T(2,128)(2,1)S(1)}, bf16[1,512]{1,0:T(2,128)(2,1)S(1)}, u32[]{:S(2)}, u32[]{:S(2)}) collective-permute-start(bf16[1,512]{1,0:T(2,128)(2,1)S(1)} %get-tuple-element.265), channel_id=1, source_target_pairs={{0,4},{4,8},{8,12},{1,5},{5,9},{9,13},{2,6},{6,10},{10,14},{3,7},{... | collective-permute-start | bytes 3080 | tf_op jit(solution)/shard_map/while/body/eval_jaxpr/ppermute | solution.py:10
  224.0 3.4 %copy-start.5 = (s32[128,4]{0,1:T(4,128)S(1)}, s32[128,4]{0,1:T(4,128)}, u32[]{:S(2)}) copy-start(s32[128,4]{0,1:T(4,128)} %param.24) | copy-start | bytes 6148
  224.0 3.7 %copy-start.6 = (f32[128,4]{0,1:T(4,128)S(1)}, f32[128,4]{0,1:T(4,128)}, u32[]{:S(2)}) copy-start(f32[128,4]{0,1:T(4,128)} %param.25) | copy-start | bytes 6148
  224.1 3.9 %copy-start.1 = (bf16[128,2048]{1,0:T(8,128)(2,1)S(1)}, bf16[128,2048]{1,0:T(8,128)(2,1)}, u32[]{:S(2)}) copy-start(bf16[128,2048]{1,0:T(8,128)(2,1)} %param.22) | copy-start | bytes 1572868
  224.1 3.9 %copy-start.4 = (f32[2048]{0:T(1024)S(1)}, f32[2048]{0:T(1024)}, u32[]{:S(2)}) copy-start(f32[2048]{0:T(1024)} %param.23) | copy-start | bytes 24580
Sparse Core Ops, SparseCore 0:
  227.5 31.0 reduce-scatter.1
where the time goes:
time: 271 us; the launch traced here: 266 us
  blocking collectives  76.9 us (28%)
  starting transfers between devices  69.2 us (26%)
  other arithmetic  31.8 us (12%)
  waiting for transfers between devices  27.8 us (10%)
  matrix products  26 us (10%)
  local copies, waits for them, and re-layouts  18.9 us (7%)
  between operations  14.5 us (5%)
    all_to_all x1, blocking collectives, experts_half(): lax.all_to_all(outgoing, ('ep', 'tp'), split_axis=0, concat_axis=0, tiled...  76.9 us
    ppermute x6, starting transfers between devices, passed_along(): return lax.ppermute(block, axis, route)  63.6 us
    ppermute x6, waiting for transfers between devices, passed_along(): return lax.ppermute(block, axis, route)  20.4 us
    another operation x4, other arithmetic  16.1 us
    gather x2, local copies, waits for them, and re-layouts, experts_half(): jnp.take(back_rows, target, axis=0).reshape(tokens, top_count, model_width)  11.7 us
    dot_general x1, matrix products, expert_rows(): jnp.dot(hidden, down_weight[0], preferred_element_type=jnp.float32)  8.14 us
    reduce_scatter x1, waiting for transfers between devices, mixer_half(): lax.psum_scatter(jnp.einsum('grsd,grde->se', attended, projection, prefer...  7.37 us
    convert_element_type x1, other arithmetic, piece_update(): weights = weights.astype(jnp.bfloat16)  6.8 us
  transfers between devices with their start and end apart: 8, of which 4 were waited for; matrix products, arithmetic and copies ran while one was open for 21% of the time, Pallas kernels for 0%

commit v1 on v0

v1 whole, which is shorter than its diff:
```python
import functools

import jax
import jax.numpy as jnp
from jax import lax
from jax.experimental import pallas as pl
from jax.experimental.pallas import tpu as pltpu
from jax.sharding import PartitionSpec as P


def stick_kernel(place_ref, query_ref, own_ref, own_bias_ref, visit_ref, visit_bias_ref, out_ref, *, distances):
    span_rows, width = query_ref.shape
    head_dim = own_ref.shape[1] // 2
    heads = width // head_dim
    tile = min(128, span_rows)
    rows_of = lax.broadcasted_iota(jnp.int32, (span_rows, span_rows), 0)
    columns_of = lax.broadcasted_iota(jnp.int32, (span_rows, span_rows), 1)
    later = (rows_of > columns_of).astype(jnp.bfloat16)

    def piece(query, keys_values, bias, kept, allowed):
        keys = keys_values[:, :head_dim]
        values = keys_values[:, head_dim:]
        logits = lax.dot_general(
            query, keys, (((1,), (1,)), ((), ())), preferred_element_type=jnp.float32
        )
        logits = logits * 0.125 + bias.astype(jnp.float32)
        keep = -(jnp.maximum(logits, 0.0) + jnp.log(1.0 + jnp.exp(-jnp.abs(logits))))
        own_log = logits + keep
        if allowed is not None:
            keep = jnp.where(allowed, keep, 0.0)
        upper = keep.astype(jnp.bfloat16)
        lower = (keep - upper.astype(jnp.float32)).astype(jnp.bfloat16)
        after = jnp.dot(upper, later, preferred_element_type=jnp.float32) + jnp.dot(
            lower, later, preferred_element_type=jnp.float32
        )
        total = own_log + after
        if kept is not None:
            total = total + kept
        weights = jnp.exp(total)
        if allowed is not None:
            weights = jnp.where(allowed, weights, 0.0)
        update = jnp.dot(
            weights.astype(jnp.bfloat16), values, preferred_element_type=jnp.float32
        )
        return update, jnp.sum(keep, axis=1, keepdims=True)

    def one_tile(index, carry):
        start = pl.multiple_of(index * tile, tile)
        query_rows = query_ref[pl.ds(start, tile), :]
        position = start + lax.broadcasted_iota(jnp.int32, (tile, span_rows), 0)
        allowed = lax.broadcasted_iota(jnp.int32, (tile, span_rows), 1) < position
        totals, kept_sums = [], []
        for head in range(heads):
            query = query_rows[:, head * head_dim : (head + 1) * head_dim]
            total, kept = piece(query, own_ref[...], own_bias_ref[...], None, allowed)
            totals.append(total)
            kept_sums.append(kept)
        state = (tuple(totals), tuple(kept_sums))
        for distance in range(1, distances + 1):

            def include(earlier, distance=distance):
                totals, kept_sums = earlier
                new_totals, new_kept = [], []
                for head in range(heads):
                    query = query_rows[:, head * head_dim : (head + 1) * head_dim]
                    update, kept = piece(
                        query,
                        visit_ref[distance - 1],
                        visit_bias_ref[distance - 1],
                        kept_sums[head],
                        None,
                    )
                    new_totals.append(totals[head] + update)
                    new_kept.append(kept_sums[head] + kept)
                return (tuple(new_totals), tuple(new_kept))

            state = lax.cond(distance <= place_ref[0], include, lambda earlier: earlier, state)
        out_ref[pl.ds(start, tile), :] = jnp.concatenate(state[0], axis=1).astype(jnp.bfloat16)
        return carry

    lax.fori_loop(0, span_rows // tile, one_tile, 0)


def attended_heads(queries, key_value, key_bias):
    span_rows, key_groups, pair_width = key_value.shape
    head_dim = pair_width // 2
    group_width = queries.shape[1] // key_groups
    axis_size = lax.axis_size("ep")
    chain_length = axis_size // max(1, axis_size // 4)
    places = [min((i + 2) % chain_length, i) for i in range(axis_size)]
    distances = max(places)
    device_place = lax.axis_index("ep")
    chain_place = jnp.minimum((device_place + 2) % chain_length, device_place)
    packed = jnp.concatenate(
        [key_value.reshape(-1, pair_width), key_bias.reshape(-1, pair_width)], axis=0
    )
    own_rows = span_rows * key_groups
    visits, visit_biases = [], []
    for distance in range(1, distances + 1):
        route = [(i - distance, i) for i in range(axis_size) if places[i] >= distance]
        got = lax.ppermute(packed, "ep", route)
        visits.append(got[:own_rows].reshape(span_rows, key_groups, pair_width))
        visit_biases.append(got[own_rows:].reshape(key_groups, span_rows))
    if not visits:
        visits, visit_biases = [key_value], [key_bias]
    visits = jnp.stack(visits)
    visit_biases = jnp.stack(visit_biases)
    place = chain_place.astype(jnp.int32).reshape(1)
    memory = pl.BlockSpec(memory_space=pltpu.VMEM)
    outputs = []
    for group in range(key_groups):
        outputs.append(
            pl.pallas_call(
                functools.partial(stick_kernel, distances=distances),
                out_shape=jax.ShapeDtypeStruct((span_rows, group_width), jnp.bfloat16),
                in_specs=[pl.BlockSpec(memory_space=pltpu.SMEM)] + [memory] * 5,
                out_specs=memory,
                name="stick",
            )(
                place,
                queries[:, group * group_width : (group + 1) * group_width],
                key_value[:, group],
                key_bias[group : group + 1],
                visits[:, :, group],
                visit_biases[:, group : group + 1],
            )
        )
    return outputs[0] if key_groups == 1 else jnp.concatenate(outputs, axis=1)


def projected(attended, out_weight):
    return lax.psum_scatter(
        jnp.dot(attended, out_weight, preferred_element_type=jnp.float32).astype(jnp.bfloat16),
        "tp",
        scatter_dimension=0,
        tiled=True,
    )


def expert_rows(arrived, gate_weight, up_weight, down_weight):
    sources, capacity, model_width = arrived.shape
    flat_rows = arrived.reshape(sources * capacity, model_width)
    gate_part = jnp.dot(flat_rows, gate_weight[0], preferred_element_type=jnp.float32)
    up_part = jnp.dot(flat_rows, up_weight[0], preferred_element_type=jnp.float32)
    hidden = (jax.nn.silu(gate_part) * up_part).astype(jnp.bfloat16)
    result = jnp.dot(hidden, down_weight[0], preferred_element_type=jnp.float32).astype(
        jnp.bfloat16
    )
    return result.reshape(sources, capacity, model_width)


def experts_and_mixer(
    queries,
    key_value,
    key_bias,
    out_weight,
    expert_input,
    norm_gain,
    routes,
    route_weights,
    gate_weight,
    up_weight,
    down_weight,
    shared_gate,
    shared_up,
    shared_down,
):
    tokens, top_count = routes.shape
    model_width = expert_input.shape[1]
    experts = lax.axis_size("ep") * lax.axis_size("tp")
    capacity = max(2, 3 * tokens * top_count // (2 * experts))
    widened = expert_input.astype(jnp.float32)
    normed = (
        widened * lax.rsqrt(jnp.mean(widened * widened, axis=-1, keepdims=True) + 1e-06) * norm_gain
    ).astype(jnp.bfloat16)
    names = jnp.arange(experts, dtype=jnp.int32)
    named = routes.T[:, None, :] == names[None, :, None]
    chosen = jnp.any(named, axis=0)
    token_weight = jnp.sum(jnp.where(named, route_weights.T[:, None, :], 0.0), axis=0)
    order = jnp.arange(tokens, dtype=jnp.int32)
    earlier = (order[:, None] < order[None, :]).astype(jnp.bfloat16)
    slots = jnp.dot(chosen.astype(jnp.bfloat16), earlier, preferred_element_type=jnp.float32)
    slots = jnp.where(chosen, slots.astype(jnp.int32), -1)
    picked = slots[:, None, :] == jnp.arange(capacity, dtype=jnp.int32)[None, :, None]
    picker = picked.astype(jnp.bfloat16).reshape(experts * capacity, tokens)
    outgoing = jnp.dot(picker, normed, preferred_element_type=jnp.float32).astype(jnp.bfloat16)
    outgoing = outgoing.reshape(experts, capacity, model_width)
    arrived = lax.all_to_all(outgoing, ("ep", "tp"), split_axis=0, concat_axis=0, tiled=True)
    attended = attended_heads(queries, key_value, key_bias)
    arrived, attended = lax.optimization_barrier((arrived, attended))
    came_back = lax.all_to_all(
        expert_rows(arrived, gate_weight, up_weight, down_weight),
        ("ep", "tp"),
        split_axis=0,
        concat_axis=0,
        tiled=True,
    )
    mixer_output = projected(attended, out_weight)
    shared_hidden = (
        jax.nn.silu(jnp.dot(normed, shared_gate, preferred_element_type=jnp.float32))
        * jnp.dot(normed, shared_up, preferred_element_type=jnp.float32)
    ).astype(jnp.bfloat16)
    shared_term = jnp.dot(shared_hidden, shared_down, preferred_element_type=jnp.float32)
    upper = token_weight.astype(jnp.bfloat16)
    lower = (token_weight - upper.astype(jnp.float32)).astype(jnp.bfloat16)
    parts = jnp.stack([upper, lower], axis=1)
    mixing = jnp.where(picked[:, :, None, :], parts[:, None], jnp.zeros((), jnp.bfloat16))
    mixing = mixing.reshape(experts * capacity, 2 * tokens)
    back_rows = came_back.reshape(experts * capacity, model_width)
    routed = lax.dot_general(
        mixing, back_rows, (((0,), (0,)), ((), ())), preferred_element_type=jnp.float32
    )
    expert_output = (routed[:tokens] + routed[tokens:] + shared_term).astype(jnp.bfloat16)
    return (mixer_output, expert_output)


def solution(mesh):
    placed = (
        P(("grp", "ep"), "tp"),
        P(("grp", "ep"), "tp", None),
        P("tp", ("grp", "ep")),
        P("tp", None),
        P(("grp", "ep", "tp"), None),
        P(),
        P(("grp", "ep", "tp"), None),
        P(("grp", "ep", "tp"), None),
        P(("ep", "tp"), None, None),
        P(("ep", "tp"), None, None),
        P(("ep", "tp"), None, None),
        P(),
        P(),
        P(),
    )
    return jax.shard_map(
        experts_and_mixer,
        mesh=mesh,
        in_specs=placed,
        out_specs=(P(("grp", "ep", "tp"), None), P(("grp", "ep", "tp"), None)),
        check_vma=False,
    )
```

time: 271 us -> 197 us (0.73)
  the two profiles are of different devices: /device:TPU:0 before, /device:TPU:15 now
where the time goes in v1:
time: 197 us; the launch traced here: 196 us
  waiting for transfers between devices  119 us (60%)
  matrix products  29.2 us (15%)
  Pallas kernels  15.8 us (8%)
  between operations  14.2 us (7%)
  starting transfers between devices  12.9 us (7%)
  other arithmetic  3 us (2%)
  local copies, waits for them, and re-layouts  2.46 us (1%)
    all_to_all x1, waiting for transfers between devices, experts_and_mixer(): lax.all_to_all(expert_rows(arrived, gate_weight, up_weight, down_weight),...  65.3 us
    ppermute x1, waiting for transfers between devices, attended_heads(): got = lax.ppermute(packed, 'ep', route)  53.4 us
    pallas_call x1, Pallas kernels, attended_heads(): pl.pallas_call(functools.partial(stick_kernel, distances=distances), out_...  15.8 us
    dot_general x1, matrix products, expert_rows(): jnp.dot(hidden, down_weight[0], preferred_element_type=jnp.float32)  8.15 us
    all_to_all x1, starting transfers between devices, experts_and_mixer(): lax.all_to_all(outgoing, ('ep', 'tp'), split_axis=0, concat_axis=0, tiled...  6.65 us
    dot_general x1, matrix products, expert_rows(): jnp.dot(flat_rows, gate_weight[0], preferred_element_type=jnp.float32)  5.48 us
    all_to_all x1, starting transfers between devices, experts_and_mixer(): lax.all_to_all(expert_rows(arrived, gate_weight, up_weight, down_weight),...  4.93 us
    dot_general x1, matrix products, experts_and_mixer(): lax.dot_general(mixing, back_rows, (((0,), (0,)), ((), ())), preferred_el...  4.24 us
  transfers between devices with their start and end apart: 4, of which 2 were waited for; matrix products, arithmetic and copies ran while one was open for 7% of the time, Pallas kernels for 8%

profile of v1, /device:TPU:15, one launch (start us, length us, event | category | flops | bytes accessed | tf_op | source)
XLA Modules:
  0.0 196.3 jit_solution(2028181289233580575)
XLA Ops:
  7.2 0.0 copy-start
  7.2 0.8 fusion.24
  8.0 0.1 fusion.9
  8.2 0.1 eq.49
  8.2 1.2 fusion.10
  9.5 0.2 bitcast_compare_fusion
  9.7 3.8 %convolution_convert_fusion.1 = bf16[768,2048]{1,0:T(8,128)(2,1)} fusion(pred[768,128]{1,0:T(32,128)(4,1)S(1)} %bitcast_compare_fusion, bf16[128,2048]{1,0:T(8,128)(2,1)} %param.18, f32[2048]{0:T(1024)} %param.19, f32[128]{0:T(128)S(1)} %add_rsqrt_fusion), kind=kOutput, calls=%fused_computation.1 | convolution fusion | flops 405274624 | bytes 3777024 | tf_op jit(solution)/shard_map/dot_general | solution.py:186
  13.4 6.7 %all-to-all-start = ((bf16[16,48,2048]{2,1,0:T(8,128)(2,1)}), bf16[16,48,2048]{2,1,0:T(8,128)(2,1)}, u32[]{:S(2)}, u32[]{:S(2)}) async-start(bf16[16,48,2048]{2,1,0:T(8,128)(2,1)} %bitcast.47), calls=%async_computation | async-start | bytes 6291456 | tf_op jit(solution)/shard_map/all_to_all | solution.py:188
  20.1 0.0 copy-done.7
  20.1 0.0 copy-done.4
  20.2 1.3 collective-permute-start
  21.5 0.0 copy-done.5
  21.5 0.8 copy.17.query_ref
  22.3 53.4 %collective-permute-done = bf16[516,128]{1,0:T(8,128)(2,1)S(1)} collective-permute-done((bf16[516,128]{1,0:T(8,128)(2,1)S(1)}, bf16[516,128]{1,0:T(8,128)(2,1)S(1)}, u32[]{:S(2)}, u32[]{:S(2)}) %collective-permute-start) | collective-permute-done | bytes 132128 | tf_op jit(solution)/shard_map/ppermute | solution.py:101
  75.7 0.6 stack_reshape.3.visit_bias_ref
  76.3 0.7 slice_bitcast_fusion.visit_ref
  77.0 15.8 %stick.1 = bf16[512,192]{1,0:T(8,128)(2,1)} custom-call(s32[1]{0:T(128)} %bitcast.3.place_ref, bf16[512,192]{1,0:T(8,128)(2,1)} %copy.17.query_ref, bf16[512,128]{1,0:T(8,128)(2,1)} %bitcast.50, bf16[1,512]{1,0:T(2,128)(2,1)} %own_bias_ref.1, bf16[1,512,128]{2,1,0:T(8,128)(2,1)} %slice_bitcast_fusion.visit_ref, bf16[1,1,512]{2,1,0:T(2,128)(2,1)} %stack_reshape.3.visit_bias_ref), custom_call_target="tpu_custom_call" | custom-call | tf_op jit(solution)/shard_map/stick/pallas_call | solution.py:113
  92.8 0.0 all-to-all-done
  92.8 5.5 %fusion.4 = f32[768,512]{1,0:T(8,128)} fusion(bf16[768,2048]{1,0:T(8,128)(2,1)} %bitcast.8, bf16[1,2048,512]{2,1,0:T(8,128)(2,1)} %param.22), kind=kOutput, calls=%fused_computation.8 | convolution fusion | flops 1610612736 | bytes 6815744 | tf_op jit(solution)/shard_map/dot_general | solution.py:143
  98.3 8.1 %convolution_convert_fusion = bf16[768,2048]{1,0:T(8,128)(2,1)} fusion(bf16[1,512,2048]{2,1,0:T(8,128)(2,1)S(1)} %copy-done, f32[768,512]{1,0:T(8,128)} %fusion.4, bf16[768,2048]{1,0:T(8,128)(2,1)} %bitcast.8, bf16[1,2048,512]{2,1,0:T(8,128)(2,1)} %param.23), kind=kOutput, calls=%fused_computation | convolution fusion | flops 3225157632 | bytes 12058624 | tf_op jit(solution)/shard_map/dot_general | solution.py:146
  106.4 4.9 %all-to-all-start.1 = ((bf16[16,48,2048]{2,1,0:T(8,128)(2,1)}), bf16[16,48,2048]{2,1,0:T(8,128)(2,1)}, u32[]{:S(2)}, u32[]{:S(2)}) async-start(bf16[16,48,2048]{2,1,0:T(8,128)(2,1)} %bitcast.48), calls=%async_computation.2 | async-start | bytes 6291456 | tf_op jit(solution)/shard_map/all_to_all | solution.py:191
  111.4 0.0 copy-start.9
  111.4 0.0 reduce-scatter.2.cloned.1.call-start
  111.4 2.0 %convolution_convert_fusion.2 = bf16[512,2048]{1,0:T(8,128)(2,1)} fusion(bf16[512,192]{1,0:T(8,128)(2,1)S(1)} %copy-done.2, bf16[192,2048]{1,0:T(8,128)(2,1)S(1)} %copy-done.3), kind=kOutput, calls=%fused_computation.2 | convolution fusion | flops 403701760 | bytes 3080192 | tf_op jit(solution)/shard_map/dot_general | solution.py:133
  113.5 0.0 reduce-scatter.2.cloned.1.call-update
  113.6 0.1 iota_compare_fusion
  113.7 0.6 broadcast_select_fusion
  114.3 0.2 copy-done.1
  114.5 1.6 fusion.30
  116.1 65.3 %all-to-all-done.1 = bf16[16,48,2048]{2,1,0:T(8,128)(2,1)} async-done(((bf16[16,48,2048]{2,1,0:T(8,128)(2,1)}), bf16[16,48,2048]{2,1,0:T(8,128)(2,1)}, u32[]{:S(2)}, u32[]{:S(2)}) %all-to-all-start.1) | async-done | bytes 3145760 | tf_op jit(solution)/shard_map/all_to_all | solution.py:191
  181.4 4.2 %fusion.15 = f32[256,2048]{1,0:T(8,128)} fusion(bf16[768,2048]{1,0:T(8,128)(2,1)} %bitcast.13, bf16[96,8,2,128]{3,2,1,0:T(2,128)(2,1)S(1)} %bitcast.49), kind=kOutput, calls=%fused_computation.22 | convolution fusion | flops 805306368 | bytes 5636096 | tf_op jit(solution)/shard_map/dot_general | solution.py:210
  185.7 3.8 %fusion = bf16[128,2048]{1,0:T(8,128)(2,1)} fusion(bf16[256,2048]{1,0:T(8,128)(2,1)} %param.27, bf16[2048,256]{1,0:T(8,128)(2,1)} %param.26, f32[256,2048]{1,0:T(8,128)} %fusion.15, f32[128,256]{1,0:T(8,128)S(1)} %fusion.30, bf16[128,2048]{1,0:T(8,128)(2,1)S(1)} %copy-done.1, f32[2048]{0:T(1024)S(1)} %copy-done.6, f32[128]{0:T(128)S(1)} %add_rsqrt_fusion), kind=kOutput, calls=%fused_computation.4 | convolution fusion | flops 270467072 | bytes 5382656 | tf_op jit(solution)/shard_map/dot_general | solution.py:203
  (24 shorter events, 0.1 us)
Async XLA Ops:
  7.2 91.1 %copy-start = (bf16[1,512,2048]{2,1,0:T(8,128)(2,1)S(1)}, bf16[1,512,2048]{2,1,0:T(8,128)(2,1)}, u32[]{:S(2)}) copy-start(bf16[1,512,2048]{2,1,0:T(8,128)(2,1)} %param.24) | copy-start | bytes 6291460
  13.4 6.7 %copy-start.7 = (bf16[1,512]{1,0:T(2,128)(2,1)S(1)}, bf16[1,512]{1,0:T(2,128)(2,1)}, u32[]{:S(2)}) copy-start(bf16[1,512]{1,0:T(2,128)(2,1)} %own_bias_ref.1) | copy-start | bytes 3076
  13.4 6.7 %copy-start.4 = (bf16[512,1,128]{2,0,1:T(8,128)(2,1)S(1)}, bf16[512,1,128]{2,0,1:T(8,128)(2,1)}, u32[]{:S(2)}) copy-start(bf16[512,1,128]{2,0,1:T(8,128)(2,1)} %param.15) | copy-start | bytes 393220
  13.4 8.0 %copy-start.5 = (bf16[512,192]{0,1:T(8,128)(2,1)S(1)}, bf16[512,192]{0,1:T(8,128)(2,1)}, u32[]{:S(2)}) copy-start(bf16[512,192]{0,1:T(8,128)(2,1)} %param.14) | copy-start | bytes 589828
  13.4 79.3 %all-to-all-start = ((bf16[16,48,2048]{2,1,0:T(8,128)(2,1)}), bf16[16,48,2048]{2,1,0:T(8,128)(2,1)}, u32[]{:S(2)}, u32[]{:S(2)}) async-start(bf16[16,48,2048]{2,1,0:T(8,128)(2,1)} %bitcast.47), calls=%async_computation | async-start | bytes 6291456 | tf_op jit(solution)/shard_map/all_to_all | solution.py:188
  20.2 55.5 %collective-permute-start = (bf16[516,128]{1,0:T(8,128)(2,1)S(1)}, bf16[516,128]{1,0:T(8,128)(2,1)S(1)}, u32[]{:S(2)}, u32[]{:S(2)}) collective-permute-start(bf16[516,128]{1,0:T(8,128)(2,1)S(1)} %pad_maximum_fusion), channel_id=1, source_target_pairs={{0,4},{8,12},{1,5},{9,13},{2,6},{10,14},{3,7},{11,15},{16,20},{24,... | collective-permute-start | bytes 396296 | tf_op jit(solution)/shard_map/ppermute | solution.py:101
  106.4 5.0 %copy-start.2 = (bf16[512,192]{1,0:T(8,128)(2,1)S(1)}, bf16[512,192]{1,0:T(8,128)(2,1)}, u32[]{:S(2)}) copy-start(bf16[512,192]{1,0:T(8,128)(2,1)} %stick.1) | copy-start | bytes 589828
  106.4 5.0 %copy-start.3 = (bf16[192,2048]{1,0:T(8,128)(2,1)S(1)}, bf16[192,2048]{1,0:T(8,128)(2,1)}, u32[]{:S(2)}) copy-start(bf16[192,2048]{1,0:T(8,128)(2,1)} %param.17) | copy-start | bytes 2359300
  106.4 75.0 %all-to-all-start.1 = ((bf16[16,48,2048]{2,1,0:T(8,128)(2,1)}), bf16[16,48,2048]{2,1,0:T(8,128)(2,1)}, u32[]{:S(2)}, u32[]{:S(2)}) async-start(bf16[16,48,2048]{2,1,0:T(8,128)(2,1)} %bitcast.48), calls=%async_computation.2 | async-start | bytes 6291456 | tf_op jit(solution)/shard_map/all_to_all | solution.py:191
  111.4 2.2 %copy-start.8 = (s32[128,4]{0,1:T(4,128)S(1)}, s32[128,4]{0,1:T(4,128)}, u32[]{:S(2)}) copy-start(s32[128,4]{0,1:T(4,128)} %param.20) | copy-start | bytes 6148
  111.4 2.2 %copy-start.9 = (f32[128,4]{0,1:T(4,128)S(1)}, f32[128,4]{0,1:T(4,128)}, u32[]{:S(2)}) copy-start(f32[128,4]{0,1:T(4,128)} %param.21) | copy-start | bytes 6148
  111.4 78.1 %reduce-scatter.2.cloned.1.call-start = ((), (), s32[]{:S(2)}) async-start(), calls=%async_computation.3 | async-start | bytes 2621440 | tf_op jit(solution)/shard_map/reduce_scatter | solution.py:132
  113.5 1.0 copy-start.1
  113.5 1.0 copy-start.6
Sparse Core Ops, SparseCore 0:
  115.3 41.2 reduce-scatter.1
